TPU v7x, 32 devices: a whole 2x2x4 slice. The times are simulated.
32 devices in a mesh: ep: 4 (over y, x), tp: 8 (over z, core).
Axes of the slice: x: 2, y: 2, z: 4, core: 2. Of those that a mesh axis runs over, the one named last changes fastest.
Arguments:
- features: bfloat16 [64, 1024], P('ep', 'tp'), may hold values from -6 to 6
- key_table: bfloat16 [65536, 1024], P('ep', 'tp'), may hold values from -0.1875 to 0.1875
- value_table: bfloat16 [65536, 1024], P('ep', 'tp'), may hold values from -6 to 6
- chosen: int32 [64, 4, 16], P('ep'), may hold values from 0 to 65535
- scores: float32 [64, 4, 16], P('ep'), may hold values from -8 to 8
Outputs:
- mixed: bfloat16 [64, 1024], P('ep', 'tp')
Inputs may be any that keep to these rules, and one draw needn't show every extreme that they name: Every chosen row is a row of the tables, 0 to 65535; rows may repeat, and a few rows are far more popular than the rest.
All inputs are finite; a program needn't handle non-finite values.
Results may differ from a plain program's by a relative error of at most 0.0065.
Values may be sent and summed in bfloat16 or wider, within the bound.
A program may use at most 64 MiB of HBM per device.

v0:
```python
import jax
import jax.numpy as jnp
from jax import lax
from jax.sharding import PartitionSpec as P


def in_blocks(func, arrays):
    total = arrays[0].shape[0]
    width = 32 if total % 32 == 0 else total
    count = total // width
    if count == 1:
        return func(arrays)
    shaped = tuple((item.reshape((count, width) + item.shape[1:]) for item in arrays))
    result = lax.map(func, shaped)
    return result.reshape((total,) + result.shape[2:])


def shards(features, key_table, value_table, chosen, scores):
    table_rows = key_table.shape[0]
    head_count = chosen.shape[1]
    top_count = chosen.shape[2]
    first_row = lax.axis_index("ep") * table_rows
    gate_weights = jax.nn.softmax(scores, axis=-1)
    chosen_all = lax.all_gather(chosen, "ep", axis=0, tiled=True)
    gates_all = lax.all_gather(gate_weights, "ep", axis=0, tiled=True)
    shifted = chosen_all - first_row
    owned_mask = (shifted >= 0) & (shifted < table_rows)
    local_rows = jnp.clip(shifted, 0, table_rows - 1).reshape(shifted.shape[0], -1)

    def dots_block(pair):
        token_block, picked = pair
        dense = lax.dot_general(
            token_block, key_table, (((1,), (1,)), ((), ())), preferred_element_type=jnp.float32
        )
        return jnp.take_along_axis(dense, picked, axis=1)

    def partial_dots(token_block):
        row_count = token_block.shape[0]
        picked = lax.slice_in_dim(local_rows, 0, row_count, axis=0)
        keep_mask = lax.slice_in_dim(owned_mask, 0, row_count, axis=0)
        products = in_blocks(dots_block, (token_block, picked))
        return jnp.where(keep_mask.reshape(row_count, -1), products, 0.0)

    partial_value = partial_dots(lax.all_gather(features, "ep", axis=0, tiled=True))
    partial_value = partial_value.reshape(-1, head_count, top_count)
    products = lax.psum(partial_value, "tp")
    row_weights = (gates_all * jax.nn.gelu(products, approximate=False)).astype(jnp.bfloat16)
    row_weights = jnp.where(owned_mask, row_weights, jnp.zeros_like(row_weights))
    flat_weights = row_weights.reshape(row_weights.shape[0], -1)

    def value_block(pair):
        block_weights, picked = pair
        width = picked.shape[0]
        token_ids = lax.broadcasted_iota(jnp.int32, picked.shape, 0)
        dense = (
            jnp.zeros((width, table_rows), jnp.float32)
            .at[token_ids, picked]
            .add(block_weights.astype(jnp.float32))
        )
        upper = dense.astype(jnp.bfloat16)
        lower = (dense - upper.astype(jnp.float32)).astype(jnp.bfloat16)
        summed = jnp.dot(upper, value_table, preferred_element_type=jnp.float32)
        return summed + jnp.dot(lower, value_table, preferred_element_type=jnp.float32)

    def owner_term(row_count):
        picked = lax.slice_in_dim(local_rows, 0, row_count, axis=0)
        block_weights = lax.slice_in_dim(flat_weights, 0, row_count, axis=0)
        return in_blocks(value_block, (block_weights, picked))

    summed = lax.psum_scatter(
        owner_term(lax.axis_size("ep") * features.shape[0]), "ep", scatter_dimension=0, tiled=True
    )
    return summed.astype(jnp.bfloat16)


def solution(mesh):
    return jax.shard_map(
        shards,
        mesh=mesh,
        in_specs=(
            P("ep", "tp"),
            P("ep", "tp"),
            P("ep", "tp"),
            P("ep", None, None),
            P("ep", None, None),
        ),
        out_specs=P("ep", "tp"),
        check_vma=False,
    )
```

profile of v0, /device:TPU:0, one launch (start us, length us, event | category | flops | bytes accessed | tf_op | source)
XLA Modules:
  0.0 150.6 jit_solution(2925781054300284029)
XLA Ops:
  0.0 10.1 %all_gather.9 = s32[64,4,16]{2,1,0:T(4,128)S(1)} all-gather(s32[16,4,16]{2,1,0:T(4,128)} %param.12), channel_id=1, replica_groups=mesh['ep'=4,'tp'=8] {'ep'}, dimensions={0}, use_global_device_ids=true | all-gather | bytes 20480 | tf_op jit(solution)/shard_map/all_gather | solution.py:24
  10.1 0.1 copy.12
  10.2 0.1 reshape_reshape.7
  10.4 8.0 %all_gather.11 = bf16[64,128]{1,0:T(8,128)(2,1)S(1)} all-gather(bf16[16,128]{1,0:T(8,128)(2,1)} %param.9), channel_id=1, replica_groups=mesh['ep'=4,'tp'=8] {'ep'}, dimensions={0}, use_global_device_ids=true | all-gather | bytes 20480 | tf_op jit(solution)/shard_map/all_gather | solution.py:44
  18.4 41.2 %while.20 = (s32[]{:T(128)}, f32[2,32,64]{2,1,0:T(8,128)S(1)}, s32[2,32,64]{2,1,0:T(8,128)S(1)}, bf16[2,32,128]{2,1,0:T(8,128)(2,1)S(1)}, bf16[16384,128]{1,0:T(8,128)(2,1)}, /*index=5*/s32[]{:T(128)}) while((s32[]{:T(128)}, f32[2,32,64]{2,1,0:T(8,128)S(1)}, s32[2,32,64]{2,1,0:T(8,128)S(1)}, bf16[2,32,128]{2,1,0:T(8,128)(2,1)S(1)}, ...), condition=%wide.region_3.4_spmd, body=%wide.region_2.3_spmd.sunk | while | flops 134248448 | bytes 6430801 | solution.py:14
  18.4 3.7 %fusion.47 = f32[32,16384]{1,0:T(8,128)S(1)} fusion(bf16[16384,128]{1,0:T(8,128)(2,1)} %get-tuple-element.181, bf16[2,32,128]{2,1,0:T(8,128)(2,1)S(1)} %get-tuple-element.180, s32[]{:T(128)} %get-tuple-element.171), kind=kOutput, calls=%fused_computation.8.clone.1 | convolution fusion | flops 134217728 | bytes 6299652 | tf_op jit(solution)/shard_map/while/body/eval_jaxpr/dot_general | solution.py:32
  22.2 16.6 %gather_fusion = f32[2048]{0:T(1024)S(1)} fusion(f32[32,16384]{1,0:T(8,128)S(1)} %fusion.47, s32[2048]{0:T(1024)S(1)} %reshape.128), kind=kCustom, calls=%fused_computation.clone.1 | custom fusion | bytes 32768 | tf_op jit(solution)/shard_map/while/body/eval_jaxpr/jit(take_along_axis)/gather | solution.py:35
  39.0 3.7 %fusion.47 = f32[32,16384]{1,0:T(8,128)S(1)} fusion(bf16[16384,128]{1,0:T(8,128)(2,1)} %get-tuple-element.181, bf16[2,32,128]{2,1,0:T(8,128)(2,1)S(1)} %get-tuple-element.180, s32[]{:T(128)} %get-tuple-element.171), kind=kOutput, calls=%fused_computation.8.clone.1 | convolution fusion | flops 134217728 | bytes 6299652 | tf_op jit(solution)/shard_map/while/body/eval_jaxpr/dot_general | solution.py:32
  42.8 16.6 %gather_fusion = f32[2048]{0:T(1024)S(1)} fusion(f32[32,16384]{1,0:T(8,128)S(1)} %fusion.47, s32[2048]{0:T(1024)S(1)} %reshape.128), kind=kCustom, calls=%fused_computation.clone.1 | custom fusion | bytes 32768 | tf_op jit(solution)/shard_map/while/body/eval_jaxpr/jit(take_along_axis)/gather | solution.py:35
  59.6 0.1 copy.14
  59.6 0.1 reshape.94
  59.8 26.0 %psum.7 = f32[64,4,16]{0,2,1:T(8,128)S(1)} all-reduce(f32[64,4,16]{0,2,1:T(8,128)S(1)} %get-tuple-element.101), channel_id=1, replica_groups=mesh['ep'=4,'tp'=8] {'tp'}, use_global_device_ids=true, to_apply=%region_4.5 | all-reduce | flops 4096 | bytes 32768 | tf_op jit(solution)/shard_map/psum | solution.py:46
  85.8 0.2 fusion.17
  86.0 7.7 %all_gather.10 = f32[64,4,16]{2,1,0:T(4,128)S(1)} all-gather(f32[16,4,16]{2,1,0:T(4,128)S(1)} %fusion.17), channel_id=1, replica_groups=mesh['ep'=4,'tp'=8] {'ep'}, dimensions={0}, use_global_device_ids=true | all-gather | bytes 20480 | tf_op jit(solution)/shard_map/all_gather | solution.py:25
  93.7 0.1 fusion.30
  93.8 0.1 reshape_reshape.8
  93.9 0.1 copy.17
  94.0 39.5 %while.21 = (s32[]{:T(128)}, f32[2,32,128]{2,1,0:T(8,128)S(1)}, s32[2,32,64]{2,1,0:T(8,128)S(1)}, bf16[2,32,64]{2,1,0:T(8,128)(2,1)S(1)}, bf16[16384,128]{1,0:T(...) while((s32[]{:T(128)}, f32[2,32,128]{2,1,0:T(8,128)S(1)}, ...), condition=%wide.region_7.8_spmd, body=%wide.region_5.7_spmd.sunk | while | flops 271101952 | bytes 35831960 | solution.py:14
  94.4 13.3 %scatter_custom_fusion.5 = f32[524288]{0:T(1024)} fusion(s32[2048]{0:T(1024)S(1)} %reshape.131, f32[2048]{0:T(1024)S(1)} %reshape.132, f32[]{:T(128)} %constant.53.clone.1..sunk), kind=kCustom, calls=%fused_computation.16.clone.1 | custom fusion | flops 2048 | bytes 2097156 | tf_op jit(solution)/shard_map/while
  107.7 1.7 %reshape.133 = f32[32,16384]{1,0:T(8,128)S(1)} reshape(f32[524288]{0:T(1024)} %scatter_custom_fusion.5) | data formatting | bytes 4194304 | tf_op jit(solution)/shard_map/while/body/eval_jaxpr/scatter-add | solution.py:58
  109.5 3.1 %fusion.53 = f32[32,128]{1,0:T(8,128)S(1)} fusion(bf16[16384,128]{1,0:T(8,128)(2,1)} %get-tuple-element.205, f32[32,16384]{1,0:T(8,128)S(1)} %reshape.133), kind=kOutput, calls=%fused_computation.19.clone.1 | convolution fusion | flops 134742016 | bytes 6307840 | tf_op jit(solution)/shard_map/while/body/eval_jaxpr/dot_general | solution.py:62
  112.6 0.3 copy-done
  112.9 0.8 fusion.54
  113.8 0.1 and_reduce_fusion.2
  114.1 13.5 %scatter_custom_fusion.5 = f32[524288]{0:T(1024)} fusion(s32[2048]{0:T(1024)S(1)} %reshape.131, f32[2048]{0:T(1024)S(1)} %reshape.132, f32[]{:T(128)} %constant.53.clone.1..sunk), kind=kCustom, calls=%fused_computation.16.clone.1 | custom fusion | flops 2048 | bytes 2097156 | tf_op jit(solution)/shard_map/while
  127.6 1.7 %reshape.133 = f32[32,16384]{1,0:T(8,128)S(1)} reshape(f32[524288]{0:T(1024)} %scatter_custom_fusion.5) | data formatting | bytes 4194304 | tf_op jit(solution)/shard_map/while/body/eval_jaxpr/scatter-add | solution.py:58
  129.3 3.1 %fusion.53 = f32[32,128]{1,0:T(8,128)S(1)} fusion(bf16[16384,128]{1,0:T(8,128)(2,1)} %get-tuple-element.205, f32[32,16384]{1,0:T(8,128)S(1)} %reshape.133), kind=kOutput, calls=%fused_computation.19.clone.1 | convolution fusion | flops 134742016 | bytes 6307840 | tf_op jit(solution)/shard_map/while/body/eval_jaxpr/dot_general | solution.py:62
  132.4 0.3 copy-done
  132.8 0.8 fusion.54
  133.6 15.1 %all-reduce = bf16[64,128]{1,0:T(8,128)(2,1)S(1)} all-reduce(f32[64,128]{1,0:T(8,128)S(1)} %bitcast.41), channel_id=2, replica_groups=mesh['ep'=4,'tp'=8] {'ep'}, use_global_device_ids=true, to_apply=%region_8.9.clone | all-reduce | flops 8192 | bytes 49152
  148.7 0.6 dynamic-slice
  150.0 0.6 dynamic-slice_convert_fusion.1
  (39 shorter events, 1.1 us)
Async XLA Ops:
  18.4 67.4 %copy-start.3 = (f32[16,4,16]{2,1,0:T(4,128)S(1)}, f32[16,4,16]{2,1,0:T(4,128)}, u32[]{:S(2)}) copy-start(f32[16,4,16]{2,1,0:T(4,128)} %param.13) | copy-start | bytes 12292
  18.4 75.6 %copy-start.1 = (s32[2]{0:T(128)S(1)}, s32[2]{0:T(128)}, u32[]{:S(2)}) copy-start(s32[2]{0:T(128)} %constant.199) | copy-start | bytes 28
  18.4 75.6 %copy-start.2 = (s32[2]{0:T(128)S(1)}, s32[2]{0:T(128)}, u32[]{:S(2)}) copy-start(s32[2]{0:T(128)} %constant.200) | copy-start | bytes 28
  94.0 54.7 %copy-start.4 = (u32[32]{0:T(128)S(1)}, u32[32]{0:T(128)}, u32[]{:S(2)}) copy-start(u32[32]{0:T(128)} %constant.148) | copy-start | bytes 388
  109.5 3.5 %copy-start = (bf16[16384,128]{1,0:T(8,128)(2,1)S(1)}, bf16[16384,128]{1,0:T(8,128)(2,1)}, u32[]{:S(2)}) copy-start(bf16[16384,128]{1,0:T(8,128)(2,1)} %get-tuple-element.205) | copy-start | bytes 12582916 | tf_op jit(solution)/shard_map/while
  129.3 3.5 %copy-start = (bf16[16384,128]{1,0:T(8,128)(2,1)S(1)}, bf16[16384,128]{1,0:T(8,128)(2,1)}, u32[]{:S(2)}) copy-start(bf16[16384,128]{1,0:T(8,128)(2,1)} %get-tuple-element.205) | copy-start | bytes 12582916 | tf_op jit(solution)/shard_map/while
where the time goes:
time: 151 us
  blocking collectives  66.9 us (44%)
  local copies, waits for them, and re-layouts  40 us (26%)
  other arithmetic  27.6 us (18%)
  matrix products  15.2 us (10%)
    gather x6, local copies, waits for them, and re-layouts, dots_block(): return jnp.take_along_axis(dense, picked, axis=1)  33.6 us
    while x8, other arithmetic  27.1 us
    psum x1, blocking collectives, shards(): products = lax.psum(partial_value, 'tp')  26 us
    unnamed x1, blocking collectives  15.1 us
    all_gather x1, blocking collectives, shards(): chosen_all = lax.all_gather(chosen, 'ep', axis=0, tiled=True)  10.1 us
    all_gather x1, blocking collectives, shards(): lax.all_gather(features, 'ep', axis=0, tiled=True)  7.96 us
    all_gather x1, blocking collectives, shards(): gates_all = lax.all_gather(gate_weights, 'ep', axis=0, tiled=True)  7.69 us
    dot_general x2, matrix products, dots_block(): lax.dot_general(token_block, key_table, (((1,), (1,)), ((), ())), preferr...  7.45 us

commit v1 on v0

--- a/solution.py
+++ b/solution.py
@@ -43,7 +43,7 @@
 
     partial_value = partial_dots(lax.all_gather(features, "ep", axis=0, tiled=True))
     partial_value = partial_value.reshape(-1, head_count, top_count)
-    products = lax.psum(partial_value, "tp")
+    products = jnp.sum(lax.all_gather(partial_value, "tp"), axis=0)
     row_weights = (gates_all * jax.nn.gelu(products, approximate=False)).astype(jnp.bfloat16)
     row_weights = jnp.where(owned_mask, row_weights, jnp.zeros_like(row_weights))
     flat_weights = row_weights.reshape(row_weights.shape[0], -1)

time: 151 us -> 143 us (0.947)
  blocking collectives: 66.9 us -> 58.4 us
    psum x1 -> x0, blocking collectives: 26 us -> none  [shards(): products = lax.psum(partial_value, 'tp')]
    all_gather x0 -> x1, blocking collectives: none -> 17.4 us  [shards(): products = jnp.sum(lax.all_gather(partial_value, 'tp'), axis=0)]
where the time goes in v1:
time: 143 us; the launch traced here: 142 us
  blocking collectives  58.4 us (41%)
  local copies, waits for them, and re-layouts  40.2 us (28%)
  other arithmetic  27.8 us (19%)
  matrix products  15.2 us (11%)
    gather x6, local copies, waits for them, and re-layouts, dots_block(): return jnp.take_along_axis(dense, picked, axis=1)  33.6 us
    while x8, other arithmetic  27.1 us
    all_gather x1, blocking collectives, shards(): products = jnp.sum(lax.all_gather(partial_value, 'tp'), axis=0)  17.4 us
    unnamed x1, blocking collectives  15.1 us
    all_gather x1, blocking collectives, shards(): chosen_all = lax.all_gather(chosen, 'ep', axis=0, tiled=True)  10.1 us
    all_gather x1, blocking collectives, shards(): lax.all_gather(features, 'ep', axis=0, tiled=True)  7.96 us
    all_gather x1, blocking collectives, shards(): gates_all = lax.all_gather(gate_weights, 'ep', axis=0, tiled=True)  7.69 us
    dot_general x2, matrix products, dots_block(): lax.dot_general(token_block, key_table, (((1,), (1,)), ((), ())), preferr...  7.43 us

profile of v1, /device:TPU:0, one launch (start us, length us, event | category | flops | bytes accessed | tf_op | source)
XLA Modules:
  0.0 142.5 jit_solution(919325881156060888)
XLA Ops:
  0.0 10.1 %all_gather.12 = s32[64,4,16]{2,1,0:T(4,128)S(1)} all-gather(s32[16,4,16]{2,1,0:T(4,128)} %param.12), channel_id=1, replica_groups=mesh['ep'=4,'tp'=8] {'ep'}, dimensions={0}, use_global_device_ids=true | all-gather | bytes 20480 | tf_op jit(solution)/shard_map/all_gather | solution.py:24
  10.2 0.1 reshape_reshape.7
  10.4 8.0 %all_gather.14 = bf16[64,128]{1,0:T(8,128)(2,1)S(1)} all-gather(bf16[16,128]{1,0:T(8,128)(2,1)} %param.9), channel_id=1, replica_groups=mesh['ep'=4,'tp'=8] {'ep'}, dimensions={0}, use_global_device_ids=true | all-gather | bytes 20480 | tf_op jit(solution)/shard_map/all_gather | solution.py:44
  18.4 41.1 %while.20 = (s32[]{:T(128)}, f32[2,32,64]{2,1,0:T(8,128)S(1)}, s32[2,32,64]{2,1,0:T(8,128)S(1)}, bf16[2,32,128]{2,1,0:T(8,128)(2,1)S(1)}, bf16[16384,128]{1,0:T(8,128)(2,1)}, /*index=5*/s32[]{:T(128)}) while((s32[]{:T(128)}, f32[2,32,64]{2,1,0:T(8,128)S(1)}, s32[2,32,64]{2,1,0:T(8,128)S(1)}, bf16[2,32,128]{2,1,0:T(8,128)(2,1)S(1)}, ...), condition=%wide.region_3.4_spmd, body=%wide.region_2.3_spmd.sunk | while | flops 134248448 | bytes 6430801 | solution.py:14
  18.4 3.7 %fusion.47 = f32[32,16384]{1,0:T(8,128)S(1)} fusion(bf16[16384,128]{1,0:T(8,128)(2,1)} %get-tuple-element.201, bf16[2,32,128]{2,1,0:T(8,128)(2,1)S(1)} %get-tuple-element.200, s32[]{:T(128)} %get-tuple-element.191), kind=kOutput, calls=%fused_computation.8.clone.1 | convolution fusion | flops 134217728 | bytes 6299652 | tf_op jit(solution)/shard_map/while/body/eval_jaxpr/dot_general | solution.py:32
  22.2 16.6 %gather_fusion = f32[2048]{0:T(1024)S(1)} fusion(f32[32,16384]{1,0:T(8,128)S(1)} %fusion.47, s32[2048]{0:T(1024)S(1)} %reshape.131), kind=kCustom, calls=%fused_computation.clone.1 | custom fusion | bytes 32768 | tf_op jit(solution)/shard_map/while/body/eval_jaxpr/jit(take_along_axis)/gather | solution.py:35
  38.9 3.7 %fusion.47 = f32[32,16384]{1,0:T(8,128)S(1)} fusion(bf16[16384,128]{1,0:T(8,128)(2,1)} %get-tuple-element.201, bf16[2,32,128]{2,1,0:T(8,128)(2,1)S(1)} %get-tuple-element.200, s32[]{:T(128)} %get-tuple-element.191), kind=kOutput, calls=%fused_computation.8.clone.1 | convolution fusion | flops 134217728 | bytes 6299652 | tf_op jit(solution)/shard_map/while/body/eval_jaxpr/dot_general | solution.py:32
  42.8 16.6 %gather_fusion = f32[2048]{0:T(1024)S(1)} fusion(f32[32,16384]{1,0:T(8,128)S(1)} %fusion.47, s32[2048]{0:T(1024)S(1)} %reshape.131), kind=kCustom, calls=%fused_computation.clone.1 | custom fusion | bytes 32768 | tf_op jit(solution)/shard_map/while/body/eval_jaxpr/jit(take_along_axis)/gather | solution.py:35
  59.5 0.1 copy.28
  59.6 0.1 reshape.96
  59.8 0.1 copy.29
  59.9 17.4 %all-gather = f32[512,4,16]{2,1,0:T(4,128)S(1)} all-gather(f32[64,4,16]{2,1,0:T(4,128)S(1)} %copy.29), channel_id=2, replica_groups=mesh['ep'=4,'tp'=8] {'tp'}, dimensions={0}, use_global_device_ids=true | all-gather | bytes 147456 | tf_op jit(solution)/shard_map/all_gather | solution.py:46
  77.3 0.3 reduce_sum.19
  77.7 0.2 fusion.17
  77.9 7.7 %all_gather.13 = f32[64,4,16]{2,1,0:T(4,128)S(1)} all-gather(f32[16,4,16]{2,1,0:T(4,128)S(1)} %fusion.17), channel_id=1, replica_groups=mesh['ep'=4,'tp'=8] {'ep'}, dimensions={0}, use_global_device_ids=true | all-gather | bytes 20480 | tf_op jit(solution)/shard_map/all_gather | solution.py:25
  85.6 0.1 fusion.30
  85.7 0.1 reshape_reshape.8
  85.8 0.1 copy.34
  85.9 39.5 %while.21 = (s32[]{:T(128)}, f32[2,32,128]{2,1,0:T(8,128)S(1)}, s32[2,32,64]{2,1,0:T(8,128)S(1)}, bf16[2,32,64]{2,1,0:T(8,128)(2,1)S(1)}, bf16[16384,128]{1,0:T(...) while((s32[]{:T(128)}, f32[2,32,128]{2,1,0:T(8,128)S(1)}, ...), condition=%wide.region_7.8_spmd, body=%wide.region_5.7_spmd.sunk | while | flops 271101952 | bytes 35831960 | solution.py:14
  86.3 13.3 %scatter_custom_fusion.5 = f32[524288]{0:T(1024)} fusion(s32[2048]{0:T(1024)S(1)} %reshape.134, f32[2048]{0:T(1024)S(1)} %reshape.135, f32[]{:T(128)} %constant.26.clone.1..sunk), kind=kCustom, calls=%fused_computation.16.clone.1 | custom fusion | flops 2048 | bytes 2097156 | tf_op jit(solution)/shard_map/while
  99.6 1.7 %reshape.136 = f32[32,16384]{1,0:T(8,128)S(1)} reshape(f32[524288]{0:T(1024)} %scatter_custom_fusion.5) | data formatting | bytes 4194304 | tf_op jit(solution)/shard_map/while/body/eval_jaxpr/scatter-add | solution.py:58
  101.4 3.1 %fusion.53 = f32[32,128]{1,0:T(8,128)S(1)} fusion(bf16[16384,128]{1,0:T(8,128)(2,1)} %get-tuple-element.225, f32[32,16384]{1,0:T(8,128)S(1)} %reshape.136), kind=kOutput, calls=%fused_computation.19.clone.1 | convolution fusion | flops 134742016 | bytes 6307840 | tf_op jit(solution)/shard_map/while/body/eval_jaxpr/dot_general | solution.py:62
  104.5 0.3 copy-done
  104.8 0.8 fusion.54
  106.0 13.5 %scatter_custom_fusion.5 = f32[524288]{0:T(1024)} fusion(s32[2048]{0:T(1024)S(1)} %reshape.134, f32[2048]{0:T(1024)S(1)} %reshape.135, f32[]{:T(128)} %constant.26.clone.1..sunk), kind=kCustom, calls=%fused_computation.16.clone.1 | custom fusion | flops 2048 | bytes 2097156 | tf_op jit(solution)/shard_map/while
  119.5 1.7 %reshape.136 = f32[32,16384]{1,0:T(8,128)S(1)} reshape(f32[524288]{0:T(1024)} %scatter_custom_fusion.5) | data formatting | bytes 4194304 | tf_op jit(solution)/shard_map/while/body/eval_jaxpr/scatter-add | solution.py:58
  121.2 3.1 %fusion.53 = f32[32,128]{1,0:T(8,128)S(1)} fusion(bf16[16384,128]{1,0:T(8,128)(2,1)} %get-tuple-element.225, f32[32,16384]{1,0:T(8,128)S(1)} %reshape.136), kind=kOutput, calls=%fused_computation.19.clone.1 | convolution fusion | flops 134742016 | bytes 6307840 | tf_op jit(solution)/shard_map/while/body/eval_jaxpr/dot_general | solution.py:62
  124.3 0.3 copy-done
  124.7 0.8 fusion.54
  125.5 15.1 %all-reduce = bf16[64,128]{1,0:T(8,128)(2,1)S(1)} all-reduce(f32[64,128]{1,0:T(8,128)S(1)} %bitcast.43), channel_id=3, replica_groups=mesh['ep'=4,'tp'=8] {'ep'}, use_global_device_ids=true, to_apply=%region_8.9.clone | all-reduce | flops 8192 | bytes 49152
  140.6 0.6 dynamic-slice
  141.9 0.6 dynamic-slice_convert_fusion.1
  (42 shorter events, 1.4 us)
Async XLA Ops:
  59.5 18.1 %copy-start.3 = (f32[16,4,16]{2,1,0:T(4,128)S(1)}, f32[16,4,16]{2,1,0:T(4,128)}, u32[]{:S(2)}) copy-start(f32[16,4,16]{2,1,0:T(4,128)} %param.13) | copy-start | bytes 12292
  59.5 26.4 %copy-start.1 = (s32[2]{0:T(128)S(1)}, s32[2]{0:T(128)}, u32[]{:S(2)}) copy-start(s32[2]{0:T(128)} %constant.199) | copy-start | bytes 28
  59.5 26.4 %copy-start.2 = (s32[2]{0:T(128)S(1)}, s32[2]{0:T(128)}, u32[]{:S(2)}) copy-start(s32[2]{0:T(128)} %constant.200) | copy-start | bytes 28
  85.9 54.7 %copy-start.4 = (u32[32]{0:T(128)S(1)}, u32[32]{0:T(128)}, u32[]{:S(2)}) copy-start(u32[32]{0:T(128)} %constant.148) | copy-start | bytes 388
  101.4 3.5 %copy-start = (bf16[16384,128]{1,0:T(8,128)(2,1)S(1)}, bf16[16384,128]{1,0:T(8,128)(2,1)}, u32[]{:S(2)}) copy-start(bf16[16384,128]{1,0:T(8,128)(2,1)} %get-tuple-element.225) | copy-start | bytes 12582916 | tf_op jit(solution)/shard_map/while
  121.2 3.5 %copy-start = (bf16[16384,128]{1,0:T(8,128)(2,1)S(1)}, bf16[16384,128]{1,0:T(8,128)(2,1)}, u32[]{:S(2)}) copy-start(bf16[16384,128]{1,0:T(8,128)(2,1)} %get-tuple-element.225) | copy-start | bytes 12582916 | tf_op jit(solution)/shard_map/while
